TPU v7x, 32 devices: a whole 2x2x4 slice. The times are simulated.
32 devices in a mesh: rep: 2 (over y), fs: 4 (over z), tp: 4 (over x, core).
Axes of the slice: x: 2, y: 2, z: 4, core: 2. Of those that a mesh axis runs over, the one named last changes fastest.
Arguments:
- stream: bfloat16 [2048, 1536], P(('rep', 'fs')), may hold values from -6 to 6
- mix_pre_gain: float32 [1536], replicated, may hold values from 0.1 to 1.9
- w_outer_gate: bfloat16 [1536, 768], P('fs', 'tp'), may hold values from -0.15625 to 0.15625
- w_inner_gate: bfloat16 [1536, 768], P('fs', 'tp'), may hold values from -0.15625 to 0.15625
- w_value: bfloat16 [1536, 768], P('fs', 'tp'), may hold values from -0.15625 to 0.15625
- mix_taps: float32 [3, 768], P(None, 'tp'), may hold values from -3 to 3
- w_mix_out: bfloat16 [768, 1536], P('tp', 'fs'), may hold values from -0.3125 to 0.3125
- mix_post_gain: float32 [1536], replicated, may hold values from 0.1 to 1.9
- ffn_pre_gain: float32 [1536], replicated, may hold values from 0.1 to 1.9
- w_linear: bfloat16 [1536, 4224], P('fs', 'tp'), may hold values from -0.15625 to 0.15625
- w_gated: bfloat16 [1536, 4224], P('fs', 'tp'), may hold values from -0.15625 to 0.15625
- ffn_taps: float32 [3, 4224], P(None, 'tp'), may hold values from -3 to 3
- ffn_bias: float32 [4224], P('tp'), may hold values from -3 to 3
- w_down: bfloat16 [4224, 1536], P('tp', 'fs'), may hold values from -0.125 to 0.125
- ffn_post_gain: float32 [1536], replicated, may hold values from 0.1 to 1.9
Outputs:
- result: bfloat16 [2048, 1536], P(('rep', 'fs'))
All inputs are finite; a program needn't handle non-finite values.
Results may differ from a plain program's by a relative error of at most 0.023.
Values may be sent and summed in bfloat16 or wider, within the bound.
A program may use at most 64 MiB of HBM per device.

v0:
```python
import jax
import jax.numpy as jnp
from jax import lax
from jax.sharding import PartitionSpec as P

SEQ_LEN = 128
EPS = 1e-06


def norm_scale(values, gain):
    return values * lax.rsqrt(jnp.mean(values * values, axis=-1, keepdims=True) + EPS) * gain


def conv_three(values, taps):
    height, breadth = values.shape
    grouped = values.reshape(height // SEQ_LEN, SEQ_LEN, breadth)
    padded = jnp.pad(grouped, ((0, 0), (1, 1), (0, 0)))
    mixed = taps[0] * padded[:, :-2] + taps[1] * padded[:, 1:-1] + taps[2] * padded[:, 2:]
    return mixed.reshape(height, breadth)


def settle(partial_value, resid, post_gain):
    branch = lax.psum(partial_value.astype(jnp.bfloat16), "tp")
    return (resid + norm_scale(branch.astype(jnp.float32), post_gain)).astype(jnp.bfloat16)


def on_device(
    stream,
    mix_pre_gain,
    w_outer_gate,
    w_inner_gate,
    w_value,
    mix_taps,
    w_mix_out,
    mix_post_gain,
    ffn_pre_gain,
    w_linear,
    w_gated,
    ffn_taps,
    ffn_bias,
    w_down,
    ffn_post_gain,
):
    resid = stream.astype(jnp.float32)
    normed = norm_scale(resid, mix_pre_gain).astype(jnp.bfloat16)
    full_outer, full_inner, full_value = (
        lax.all_gather(w_outer_gate, "fs", axis=0, tiled=True),
        lax.all_gather(w_inner_gate, "fs", axis=0, tiled=True),
        lax.all_gather(w_value, "fs", axis=0, tiled=True),
    )
    outer = jnp.dot(normed, full_outer, preferred_element_type=jnp.float32)
    inner = jnp.dot(normed, full_inner, preferred_element_type=jnp.float32)
    value = jnp.dot(normed, full_value, preferred_element_type=jnp.float32)
    outer = outer.astype(jnp.bfloat16)
    inner = inner.astype(jnp.bfloat16)
    value = value.astype(jnp.bfloat16)
    product = inner.astype(jnp.float32) * value.astype(jnp.float32)
    mixed = (outer.astype(jnp.float32) * conv_three(product, mix_taps)).astype(jnp.bfloat16)
    full_mix_out = lax.all_gather(w_mix_out, "fs", axis=1, tiled=True)
    partial_value = jnp.dot(mixed, full_mix_out, preferred_element_type=jnp.float32)
    middle = settle(partial_value, resid, mix_post_gain)
    middle_f = middle.astype(jnp.float32)
    normed_two = norm_scale(middle_f, ffn_pre_gain).astype(jnp.bfloat16)
    full_linear, full_gated = (
        lax.all_gather(w_linear, "fs", axis=0, tiled=True),
        lax.all_gather(w_gated, "fs", axis=0, tiled=True),
    )
    linear = jnp.dot(normed_two, full_linear, preferred_element_type=jnp.float32)
    gated = jnp.dot(normed_two, full_gated, preferred_element_type=jnp.float32)
    linear = linear.astype(jnp.bfloat16)
    gated = gated.astype(jnp.bfloat16)
    activated = jax.nn.gelu(
        conv_three(gated.astype(jnp.float32), ffn_taps) + ffn_bias, approximate=True
    )
    hidden = (activated * linear.astype(jnp.float32)).astype(jnp.bfloat16)
    full_down = lax.all_gather(w_down, "fs", axis=1, tiled=True)
    partial_two = jnp.dot(hidden, full_down, preferred_element_type=jnp.float32)
    return settle(partial_two, middle_f, ffn_post_gain)


def solution(mesh):
    in_specs = (
        P(("rep", "fs"), None),
        P(),
        P("fs", "tp"),
        P("fs", "tp"),
        P("fs", "tp"),
        P(None, "tp"),
        P("tp", "fs"),
        P(),
        P(),
        P("fs", "tp"),
        P("fs", "tp"),
        P(None, "tp"),
        P("tp"),
        P("tp", "fs"),
        P(),
    )
    out_specs = P(("rep", "fs"), None)
    return jax.shard_map(
        on_device, mesh=mesh, in_specs=in_specs, out_specs=out_specs, check_vma=False
    )
```

profile of v0, /device:TPU:0, one launch (start us, length us, event | category | flops | bytes accessed | tf_op | source)
XLA Modules:
  0.0 331.4 jit_solution(645357725762932306)
XLA Ops:
  7.4 1.5 fusion.8
  8.8 18.7 %all_gather.22 = bf16[1536,192]{0,1:T(8,128)(2,1)S(1)} all-gather(bf16[384,192]{0,1:T(8,128)(2,1)} %param.18), channel_id=1, replica_groups=mesh['rep'=2,'fs'=4,'tp'=4] {'fs'}, dimensions={0}, use_global_device_ids=true | all-gather | bytes 737280 | tf_op jit(solution)/shard_map/all_gather | solution.py:48
  27.5 16.1 %all_gather.23 = bf16[1536,192]{0,1:T(8,128)(2,1)S(1)} all-gather(bf16[384,192]{0,1:T(8,128)(2,1)S(1)} %copy-done.1), channel_id=1, replica_groups=mesh['rep'=2,'fs'=4,'tp'=4] {'fs'}, dimensions={0}, use_global_device_ids=true | all-gather | bytes 737280 | tf_op jit(solution)/shard_map/all_gather | solution.py:49
  44.2 0.5 fusion.17
  45.1 16.4 %all_gather.21 = bf16[1536,192]{0,1:T(8,128)(2,1)S(1)} all-gather(bf16[384,192]{0,1:T(8,128)(2,1)S(1)} %copy-done.2), channel_id=1, replica_groups=mesh['rep'=2,'fs'=4,'tp'=4] {'fs'}, dimensions={0}, use_global_device_ids=true | all-gather | bytes 737280 | tf_op jit(solution)/shard_map/all_gather | solution.py:47
  61.5 15.5 %all_gather.24 = bf16[192,1536]{1,0:T(8,128)(2,1)S(1)} all-gather(bf16[192,384]{1,0:T(8,128)(2,1)S(1)} %copy-done.3), channel_id=1, replica_groups=mesh['rep'=2,'fs'=4,'tp'=4] {'fs'}, dimensions={1}, use_global_device_ids=true | all-gather | bytes 737280 | tf_op jit(solution)/shard_map/all_gather | solution.py:59
  77.0 1.2 fusion.43
  78.2 2.1 convolution_convert_fusion.3
  80.4 0.5 all-gather.4.cloned.1.call-update
  81.0 0.5 all-gather.6.cloned.1.call-update
  81.6 0.5 all-gather.8.cloned.1.call-update
  82.2 34.8 %all-reduce.5.cloned.1.call-done = bf16[256,1536]{1,0:T(8,128)(2,1)} async-done(((bf16[256,1536]{1,0:T(8,128)(2,1)}), bf16[256,1536]{1,0:T(8,128)(2,1)}) %all-reduce.5.cloned.1.call-update) | async-done | bytes 786448 | tf_op jit(solution)/shard_map/psum | solution.py:23
  117.0 1.4 fusion.4
  118.4 1.7 fusion.12
  120.1 28.7 %all-gather.4.cloned.1.call-done = bf16[1536,1056]{0,1:T(8,128)(2,1)} async-done(((bf16[384,1056]{0,1:T(8,128)(2,1)}), bf16[1536,1056]{0,1:T(8,128)(2,1)}) %all-gather.4.cloned.1.call-update) | async-done | bytes 3244048 | tf_op jit(solution)/shard_map/all_gather | solution.py:66
  148.7 4.0 %fusion.2 = f32[256,1056]{0,1:T(8,128)} fusion(bf16[1536,1056]{0,1:T(8,128)(2,1)} %all-gather.4.cloned.1.call-done, bf16[256,1536]{1,0:T(8,128)(2,1)S(1)} %get-tuple-element.9, f32[1536]{0:T(1024)S(1)} %copy-done.9, f32[256]{0:T(256)S(1)} %add_rsqrt_fusion.1), kind=kOutput, calls=%fused_computation.4 | convolution fusion | flops 832585728 | bytes 5118976 | tf_op jit(solution)/shard_map/dot_general | solution.py:69
  152.8 1.8 reshape.64
  154.6 7.3 %fusion.31 = f32[2,128,1056]{1,0,2:T(2,128)} fusion(f32[2,128,1056]{1,0,2:T(2,128)S(1)} %reshape.64, f32[1056]{0:T(1024)S(1)} %get-tuple-element.6, f32[1056]{0:T(1024)S(1)} %get-tuple-element.7, f32[1056]{0:T(1024)S(1)} %get-tuple-element.5), kind=kLoop, calls=%fused_computation.51 | loop fusion | flops 1351680 | bytes 2175360 | tf_op jit(solution)/shard_map/add | solution.py:18
  162.0 51.6 %all-gather.6.cloned.1.call-done = bf16[1536,1056]{0,1:T(8,128)(2,1)} async-done(((bf16[384,1056]{0,1:T(8,128)(2,1)}), bf16[1536,1056]{0,1:T(8,128)(2,1)}) %all-gather.6.cloned.1.call-update) | async-done | bytes 3244048 | tf_op jit(solution)/shard_map/all_gather | solution.py:65
  213.5 64.8 %all-gather.8.cloned.1.call-done = bf16[1056,1536]{1,0:T(8,128)(2,1)} async-done(((bf16[1056,384]{1,0:T(8,128)(2,1)}), bf16[1056,1536]{1,0:T(8,128)(2,1)}) %all-gather.8.cloned.1.call-update) | async-done | bytes 3244048 | tf_op jit(solution)/shard_map/all_gather | solution.py:76
  278.3 7.9 %convolution_convert_fusion.2 = bf16[256,1536]{1,0:T(8,128)(2,1)} fusion(bf16[1056,1536]{1,0:T(8,128)(2,1)} %all-gather.8.cloned.1.call-done, bf16[1536,1056]{0,1:T(8,128)(2,1)} %all-gather.6.cloned.1.call-done, f32[132,8,2,128]{3,2,1,0:T(2,128)} %bitcast.31, f32[1056]{0:T(1024)S(1)} %copy-done.10, bf16[256,1536]{1,0:T(8,128)(2,1)S(1)} %get-tuple-element.9, ...), kind=kOutput, calls=%fused_computation.6 | convolution fusion | flops 1666424832 | bytes 9153664 | tf_op jit(solution)/shard_map/dot_general | solution.py:77
  286.3 33.8 %all-reduce.7.cloned.1.call-done = bf16[256,1536]{1,0:T(8,128)(2,1)} async-done(((bf16[256,1536]{1,0:T(8,128)(2,1)}), bf16[256,1536]{1,0:T(8,128)(2,1)}) %all-reduce.7.cloned.1.call-update) | async-done | bytes 786448 | tf_op jit(solution)/shard_map/psum | solution.py:23
  320.1 1.4 fusion.6
  321.5 2.4 fusion.15
  (37 shorter events, 1.2 us)
Async XLA Ops:
  7.4 36.3 %copy-start = (bf16[256,1536]{1,0:T(8,128)(2,1)S(1)}, bf16[256,1536]{1,0:T(8,128)(2,1)}, u32[]{:S(2)}) copy-start(bf16[256,1536]{1,0:T(8,128)(2,1)} %param.15) | copy-start | bytes 2359300
  7.4 20.2 %copy-start.1 = (bf16[384,192]{0,1:T(8,128)(2,1)S(1)}, bf16[384,192]{0,1:T(8,128)(2,1)}, u32[]{:S(2)}) copy-start(bf16[384,192]{0,1:T(8,128)(2,1)} %param.19) | copy-start | bytes 442372
  7.4 36.3 %copy-start.8 = (f32[1536]{0:T(1024)S(1)}, f32[1536]{0:T(1024)}, u32[]{:S(2)}) copy-start(f32[1536]{0:T(1024)} %param.16) | copy-start | bytes 18436
  7.4 109.6 %all-reduce.5.cloned.1.call-start = ((), (), s32[]{:S(2)}) async-start(), calls=%async_computation | async-start | bytes 1572864 | tf_op jit(solution)/shard_map/psum | solution.py:23
  44.2 0.7 copy-start.7
  44.2 0.9 copy-start.2
  44.2 17.3 %copy-start.3 = (bf16[192,384]{1,0:T(8,128)(2,1)S(1)}, bf16[192,384]{1,0:T(8,128)(2,1)}, u32[]{:S(2)}) copy-start(bf16[192,384]{1,0:T(8,128)(2,1)} %param.21) | copy-start | bytes 442372
  80.3 1.8 copy-start.4
  80.4 38.0 %copy-start.5 = (f32[1536]{0:T(1024)S(1)}, f32[1536]{0:T(1024)}, u32[]{:S(2)}) copy-start(f32[1536]{0:T(1024)} %param.22) | copy-start | bytes 18436
  80.4 68.4 %all-gather.4.cloned.1.call-start = ((), (), s32[]{:S(2)}) async-start(), calls=%async_computation.1 | async-start | bytes 4055040 | tf_op jit(solution)/shard_map/all_gather | solution.py:66
  80.9 132.6 %all-gather.6.cloned.1.call-start = ((), (), s32[]{:S(2)}) async-start(), calls=%async_computation.2 | async-start | bytes 4055040 | tf_op jit(solution)/shard_map/all_gather | solution.py:65
  81.5 196.8 %all-gather.8.cloned.1.call-start = ((), (), s32[]{:S(2)}) async-start(), calls=%async_computation.3 | async-start | bytes 4055040 | tf_op jit(solution)/shard_map/all_gather | solution.py:76
  82.1 238.0 %all-reduce.7.cloned.1.call-start = ((), (), s32[]{:S(2)}) async-start(), calls=%async_computation.4 | async-start | bytes 1572864 | tf_op jit(solution)/shard_map/psum | solution.py:23
  82.2 66.5 %copy-start.9 = (f32[1536]{0:T(1024)S(1)}, f32[1536]{0:T(1024)}, u32[]{:S(2)}) copy-start(f32[1536]{0:T(1024)} %param.23) | copy-start | bytes 18436
  154.6 123.7 %copy-start.10 = (f32[1056]{0:T(1024)S(1)}, f32[1056]{0:T(1024)}, u32[]{:S(2)}) copy-start(f32[1056]{0:T(1024)} %param.27) | copy-start | bytes 12676
  286.3 35.2 %copy-start.6 = (f32[1536]{0:T(1024)S(1)}, f32[1536]{0:T(1024)}, u32[]{:S(2)}) copy-start(f32[1536]{0:T(1024)} %param.29) | copy-start | bytes 18436
Sparse Core Ops, SparseCore 0:
  80.5 36.4 all-reduce.4
  286.4 33.6 all-reduce.6
Sparse Core Ops, SparseCore 1:
  82.4 66.2 all-gather.3
  150.2 63.3 all-gather.5
  215.0 63.3 all-gather.7
where the time goes:
time: 332 us; the launch traced here: 331 us
  waiting for transfers between devices  215 us (65%)
  blocking collectives  66.7 us (20%)
  other arithmetic  16.8 us (5%)
  between operations  15.2 us (5%)
  matrix products  15.1 us (5%)
    psum x2, waiting for transfers between devices, settle(): branch = lax.psum(partial_value.astype(jnp.bfloat16), 'tp')  68.6 us
    all_gather x1, waiting for transfers between devices, on_device(): full_down = lax.all_gather(w_down, 'fs', axis=1, tiled=True)  64.8 us
    all_gather x1, waiting for transfers between devices, on_device(): lax.all_gather(w_linear, 'fs', axis=0, tiled=True)  51.6 us
    all_gather x1, waiting for transfers between devices, on_device(): lax.all_gather(w_gated, 'fs', axis=0, tiled=True)  28.7 us
    all_gather x1, blocking collectives, on_device(): lax.all_gather(w_inner_gate, 'fs', axis=0, tiled=True)  18.7 us
    all_gather x1, blocking collectives, on_device(): lax.all_gather(w_outer_gate, 'fs', axis=0, tiled=True)  16.4 us
    all_gather x1, blocking collectives, on_device(): lax.all_gather(w_value, 'fs', axis=0, tiled=True)  16.1 us
    all_gather x1, blocking collectives, on_device(): full_mix_out = lax.all_gather(w_mix_out, 'fs', axis=1, tiled=True)  15.5 us
  transfers between devices with their start and end apart: 5, of which 5 were waited for; matrix products, arithmetic and copies ran while one was open for 5% of the time, Pallas kernels for 0%

commit v1 on v0

--- a/solution.py
+++ b/solution.py
@@ -5,6 +5,16 @@
 
 SEQ_LEN = 128
 EPS = 1e-06
+
+
+def gather_by_hops(x, name, dim):
+    size = lax.axis_size(name)
+    current, tiles = (x, [x])
+    for _ in range(size - 1):
+        current = lax.ppermute(current, name, [(i, (i + 1) % size) for i in range(size)])
+        tiles.insert(0, current)
+    row_of_blocks = jnp.concatenate(tiles, axis=dim)
+    return jnp.roll(row_of_blocks, (lax.axis_index(name) + 1) * x.shape[dim], axis=dim)
 
 
 def norm_scale(values, gain):
@@ -73,7 +83,7 @@
         conv_three(gated.astype(jnp.float32), ffn_taps) + ffn_bias, approximate=True
     )
     hidden = (activated * linear.astype(jnp.float32)).astype(jnp.bfloat16)
-    full_down = lax.all_gather(w_down, "fs", axis=1, tiled=True)
+    full_down = gather_by_hops(w_down, "fs", 1)
     partial_two = jnp.dot(hidden, full_down, preferred_element_type=jnp.float32)
     return settle(partial_two, middle_f, ffn_post_gain)
 

time: 332 us -> 294 us (0.89)
  waiting for transfers between devices: 215 us -> 139 us
  starting transfers between devices: 0.17 us -> 31.1 us
  local copies, waits for them, and re-layouts: 2.28 us -> 9.73 us
    ppermute x0 -> x3, waiting for transfers between devices: none -> 66.6 us  [gather_by_hops(): lax.ppermute(current, name, [(i, (i + 1) % size) for i in range(size)])]
    all_gather x1 -> x0, waiting for transfers between devices: 64.8 us -> none  [on_device(): full_down = lax.all_gather(w_down, 'fs', axis=1, tiled=True)]
    psum x2, waiting for transfers between devices: 68.6 us -> 33.8 us  [settle(): branch = lax.psum(partial_value.astype(jnp.bfloat16), 'tp')]
    ppermute x0 -> x3, starting transfers between devices: none -> 31 us  [gather_by_hops(): lax.ppermute(current, name, [(i, (i + 1) % size) for i in range(size)])]
    all_gather x1, waiting for transfers between devices: 28.7 us -> 0.01 us  [on_device(): lax.all_gather(w_gated, 'fs', axis=0, tiled=True)]
    all_gather x1, waiting for transfers between devices: 51.6 us -> 38.4 us  [on_device(): lax.all_gather(w_linear, 'fs', axis=0, tiled=True)]
    unnamed x22 -> x31, local copies, waits for them, and re-layouts: 0.32 us -> 7.97 us
    all_gather x1, blocking collectives: 15.5 us -> 18.8 us  [on_device(): full_mix_out = lax.all_gather(w_mix_out, 'fs', axis=1, tiled=True)]
  transfers between devices with their start and end apart: 5 -> 7, of which waited for: 5 -> 5; matrix products, arithmetic and copies ran while one was open for 5% -> 8% of each run, Pallas kernels for 0% -> 0%
where the time goes in v1:
time: 294 us; the launch traced here: 293 us
  waiting for transfers between devices  139 us (47%)
  blocking collectives  68.3 us (23%)
  starting transfers between devices  31.1 us (11%)
  other arithmetic  15.7 us (5%)
  between operations  15 us (5%)
  matrix products  14 us (5%)
  local copies, waits for them, and re-layouts  9.73 us (3%)
    ppermute x3, waiting for transfers between devices, gather_by_hops(): lax.ppermute(current, name, [(i, (i + 1) % size) for i in range(size)])  66.6 us
    all_gather x1, waiting for transfers between devices, on_device(): lax.all_gather(w_linear, 'fs', axis=0, tiled=True)  38.4 us
    psum x2, waiting for transfers between devices, settle(): branch = lax.psum(partial_value.astype(jnp.bfloat16), 'tp')  33.8 us
    ppermute x3, starting transfers between devices, gather_by_hops(): lax.ppermute(current, name, [(i, (i + 1) % size) for i in range(size)])  31 us
    all_gather x1, blocking collectives, on_device(): full_mix_out = lax.all_gather(w_mix_out, 'fs', axis=1, tiled=True)  18.8 us
    all_gather x1, blocking collectives, on_device(): lax.all_gather(w_outer_gate, 'fs', axis=0, tiled=True)  17.3 us
    all_gather x1, blocking collectives, on_device(): lax.all_gather(w_value, 'fs', axis=0, tiled=True)  16.1 us
    all_gather x1, blocking collectives, on_device(): lax.all_gather(w_inner_gate, 'fs', axis=0, tiled=True)  16 us
  transfers between devices with their start and end apart: 7, of which 5 were waited for; matrix products, arithmetic and copies ran while one was open for 8% of the time, Pallas kernels for 0%

profile of v1, /device:TPU:0, one launch (start us, length us, event | category | flops | bytes accessed | tf_op | source)
XLA Modules:
  0.0 293.1 jit_solution(7228122063508324441)
XLA Ops:
  7.4 18.8 %all_gather.21 = bf16[192,1536]{1,0:T(8,128)(2,1)S(1)} all-gather(bf16[192,384]{1,0:T(8,128)(2,1)} %param.21), channel_id=1, replica_groups=mesh['rep'=2,'fs'=4,'tp'=4] {'fs'}, dimensions={1}, use_global_device_ids=true | all-gather | bytes 737280 | tf_op jit(solution)/shard_map/all_gather | solution.py:69
  26.2 17.3 %all_gather.18 = bf16[1536,192]{0,1:T(8,128)(2,1)S(1)} all-gather(bf16[384,192]{0,1:T(8,128)(2,1)} %param.17), channel_id=1, replica_groups=mesh['rep'=2,'fs'=4,'tp'=4] {'fs'}, dimensions={0}, use_global_device_ids=true | all-gather | bytes 737280 | tf_op jit(solution)/shard_map/all_gather | solution.py:57
  43.5 16.0 %all_gather.19 = bf16[1536,192]{0,1:T(8,128)(2,1)S(1)} all-gather(bf16[384,192]{0,1:T(8,128)(2,1)S(1)} %copy-done.3), channel_id=1, replica_groups=mesh['rep'=2,'fs'=4,'tp'=4] {'fs'}, dimensions={0}, use_global_device_ids=true | all-gather | bytes 737280 | tf_op jit(solution)/shard_map/all_gather | solution.py:58
  59.8 16.1 %all_gather.20 = bf16[1536,192]{0,1:T(8,128)(2,1)S(1)} all-gather(bf16[384,192]{0,1:T(8,128)(2,1)S(1)} %copy-done.4), channel_id=1, replica_groups=mesh['rep'=2,'fs'=4,'tp'=4] {'fs'}, dimensions={0}, use_global_device_ids=true | all-gather | bytes 737280 | tf_op jit(solution)/shard_map/all_gather | solution.py:59
  77.1 1.2 fusion.48
  78.3 2.1 convolution_convert_fusion.2
  81.6 8.4 %collective-permute-start = (bf16[1056,384]{1,0:T(8,128)(2,1)S(1)}, bf16[1056,384]{1,0:T(8,128)(2,1)S(1)}, u32[]{:S(2)}, u32[]{:S(2)}) collective-permute-start(bf16[1056,384]{1,0:T(8,128)(2,1)S(1)} %copy-done), channel_id=1, source_target_pairs={{0,4},{4,8},{8,12},{12,0},{1,5},{5,9},{9,13},{13,1},{2,6},{6,10},{... | collective-permute-start | bytes 2433032 | tf_op jit(solution)/shard_map/ppermute | solution.py:14
  90.1 19.6 %collective-permute-done = bf16[1056,384]{1,0:T(8,128)(2,1)S(1)} collective-permute-done((bf16[1056,384]{1,0:T(8,128)(2,1)S(1)}, bf16[1056,384]{1,0:T(8,128)(2,1)S(1)}, u32[]{:S(2)}, u32[]{:S(2)}) %collective-permute-start) | collective-permute-done | bytes 811040 | tf_op jit(solution)/shard_map/ppermute | solution.py:14
  109.7 5.5 %collective-permute-start.1 = (bf16[1056,384]{1,0:T(8,128)(2,1)S(1)}, bf16[1056,384]{1,0:T(8,128)(2,1)S(1)}, u32[]{:S(2)}, u32[]{:S(2)}) collective-permute-start(bf16[1056,384]{1,0:T(8,128)(2,1)S(1)} %collective-permute-done), channel_id=1, source_target_pairs={{0,4},{4,8},{8,12},{12,0},{1,5},{5,9},{9,13},{13,1},{2,6},{6,10},{... | collective-permute-start | bytes 2433032 | tf_op jit(solution)/shard_map/ppermute | solution.py:14
  115.2 36.1 %collective-permute-done.1 = bf16[1056,384]{1,0:T(8,128)(2,1)S(1)} collective-permute-done((bf16[1056,384]{1,0:T(8,128)(2,1)S(1)}, bf16[1056,384]{1,0:T(8,128)(2,1)S(1)}, u32[]{:S(2)}, u32[]{:S(2)}) %collective-permute-start.1) | collective-permute-done | bytes 811040 | tf_op jit(solution)/shard_map/ppermute | solution.py:14
  151.3 17.1 %collective-permute-start.2 = (bf16[1056,384]{1,0:T(8,128)(2,1)S(1)}, bf16[1056,384]{1,0:T(8,128)(2,1)S(1)}, u32[]{:S(2)}, u32[]{:S(2)}) collective-permute-start(bf16[1056,384]{1,0:T(8,128)(2,1)S(1)} %collective-permute-done.1), channel_id=1, source_target_pairs={{0,4},{4,8},{8,12},{12,0},{1,5},{5,9},{9,13},{13,1},{2,6},{6,10},{... | collective-permute-start | bytes 2433032 | tf_op jit(solution)/shard_map/ppermute | solution.py:14
  168.4 1.4 fusion.9
  169.8 2.7 fusion.17
  172.5 10.9 %collective-permute-done.2 = bf16[1056,384]{1,0:T(8,128)(2,1)S(1)} collective-permute-done((bf16[1056,384]{1,0:T(8,128)(2,1)S(1)}, bf16[1056,384]{1,0:T(8,128)(2,1)S(1)}, u32[]{:S(2)}, u32[]{:S(2)}) %collective-permute-start.2) | collective-permute-done | bytes 811040 | tf_op jit(solution)/shard_map/ppermute | solution.py:14
  183.4 1.1 constant_dynamic-update-slice_fusion.7
  184.4 1.1 constant_dynamic-update-slice_fusion.6
  190.7 1.1 constant_dynamic-update-slice_fusion
  191.8 3.0 %fusion.4 = f32[256,1056]{0,1:T(8,128)S(1)} fusion(bf16[1536,1056]{0,1:T(8,128)(2,1)} %all-gather.3.cloned.1.call-done, bf16[256,1536]{1,0:T(8,128)(2,1)S(1)} %copy-done.2, f32[1536]{0:T(1024)S(1)} %copy-done.10, f32[256]{0:T(256)S(1)} %add_rsqrt_fusion.1), kind=kOutput, calls=%fused_computation.6 | convolution fusion | flops 832585728 | bytes 5118976 | tf_op jit(solution)/shard_map/dot_general | solution.py:79
  195.4 6.5 %fusion.36 = f32[2,128,1056]{1,0,2:T(2,128)S(1)} fusion(f32[2,128,1056]{1,0,2:T(2,128)S(1)} %reshape.64, f32[1056]{0:T(1024)S(1)} %get-tuple-element.6, f32[1056]{0:T(1024)S(1)} %get-tuple-element.7, f32[1056]{0:T(1024)S(1)} %get-tuple-element.5), kind=kLoop, calls=%fused_computation.53 | loop fusion | flops 1351680 | bytes 2175360 | tf_op jit(solution)/shard_map/add | solution.py:28
  201.9 38.4 %all-gather.5.cloned.1.call-done = bf16[1536,1056]{0,1:T(8,128)(2,1)} async-done(((bf16[384,1056]{0,1:T(8,128)(2,1)}), bf16[1536,1056]{0,1:T(8,128)(2,1)}) %all-gather.5.cloned.1.call-update) | async-done | bytes 3244048 | tf_op jit(solution)/shard_map/all_gather | solution.py:75
  240.3 7.8 %fusion.6 = bf16[256,1536]{1,0:T(8,128)(2,1)} fusion(bf16[1056,3072]{1,0:T(8,128)(2,1)} %constant_dynamic-update-slice_fusion, s32[]{:T(128)S(6)} %select_n.14, bf16[1536,1056]{0,1:T(8,128)(2,1)} %all-gather.5.cloned.1.call-done, f32[132,8,2,128]{3,2,1,0:T(2,128)S(1)} %bitcast.30, f32[1056]{0:T(1024)S(1)} %copy-done.11, bf16[256,1536]{1,0:T(8,128)(2,1)S(1)} %copy-done.2, ...), kind=kOutput, calls=%fused_computation.8 | convolution fusion | flops 1666424832 | bytes 9153668 | tf_op jit(solution)/shard_map/dot_general | solution.py:87
  248.2 33.8 %all-reduce.7.cloned.1.call-done = bf16[256,1536]{1,0:T(8,128)(2,1)} async-done(((bf16[256,1536]{1,0:T(8,128)(2,1)}), bf16[256,1536]{1,0:T(8,128)(2,1)}) %all-reduce.7.cloned.1.call-update) | async-done | bytes 786448 | tf_op jit(solution)/shard_map/psum | solution.py:33
  282.0 1.4 fusion.11
  283.4 2.4 fusion.20
  (50 shorter events, 8.5 us)
Async XLA Ops:
  7.4 36.2 %copy-start.3 = (bf16[384,192]{0,1:T(8,128)(2,1)S(1)}, bf16[384,192]{0,1:T(8,128)(2,1)}, u32[]{:S(2)}) copy-start(bf16[384,192]{0,1:T(8,128)(2,1)} %param.18) | copy-start | bytes 442372
  7.4 52.2 %copy-start.1 = (bf16[256,1536]{1,0:T(8,128)(2,1)S(1)}, bf16[256,1536]{1,0:T(8,128)(2,1)}, u32[]{:S(2)}) copy-start(bf16[256,1536]{1,0:T(8,128)(2,1)} %param.15) | copy-start | bytes 2359300
  7.4 52.4 %copy-start.4 = (bf16[384,192]{0,1:T(8,128)(2,1)S(1)}, bf16[384,192]{0,1:T(8,128)(2,1)}, u32[]{:S(2)}) copy-start(bf16[384,192]{0,1:T(8,128)(2,1)} %param.19) | copy-start | bytes 442372
  7.4 161.0 %all-reduce.5.cloned.1.call-start = ((), (), s32[]{:S(2)}) async-start(), calls=%async_computation | async-start | bytes 1572864 | tf_op jit(solution)/shard_map/psum | solution.py:33
  26.2 49.7 %copy-start.9 = (f32[1536]{0:T(1024)S(1)}, f32[1536]{0:T(1024)}, u32[]{:S(2)}) copy-start(f32[1536]{0:T(1024)} %param.16) | copy-start | bytes 18436
  76.5 0.7 copy-start.8
  80.5 1.1 copy-start
  80.5 34.7 %copy-start.5 = (f32[3,1056]{1,0:T(4,128)S(1)}, f32[3,1056]{1,0:T(4,128)}, u32[]{:S(2)}) copy-start(f32[3,1056]{1,0:T(4,128)} %param.26) | copy-start | bytes 38020
  80.5 89.3 %copy-start.6 = (f32[1536]{0:T(1024)S(1)}, f32[1536]{0:T(1024)}, u32[]{:S(2)}) copy-start(f32[1536]{0:T(1024)} %param.22) | copy-start | bytes 18436
  80.5 111.3 %all-gather.3.cloned.1.call-start = ((), (), s32[]{:S(2)}) async-start(), calls=%async_computation.1 | async-start | bytes 4055040 | tf_op jit(solution)/shard_map/all_gather | solution.py:76
  81.1 159.3 %all-gather.5.cloned.1.call-start = ((), (), s32[]{:S(2)}) async-start(), calls=%async_computation.2 | async-start | bytes 4055040 | tf_op jit(solution)/shard_map/all_gather | solution.py:75
  81.6 28.1 %collective-permute-start = (bf16[1056,384]{1,0:T(8,128)(2,1)S(1)}, bf16[1056,384]{1,0:T(8,128)(2,1)S(1)}, u32[]{:S(2)}, u32[]{:S(2)}) collective-permute-start(bf16[1056,384]{1,0:T(8,128)(2,1)S(1)} %copy-done), channel_id=1, source_target_pairs={{0,4},{4,8},{8,12},{12,0},{1,5},{5,9},{9,13},{13,1},{2,6},{6,10},{... | collective-permute-start | bytes 2433032 | tf_op jit(solution)/shard_map/ppermute | solution.py:14
  90.0 191.9 %all-reduce.7.cloned.1.call-start = ((), (), s32[]{:S(2)}) async-start(), calls=%async_computation.3 | async-start | bytes 1572864 | tf_op jit(solution)/shard_map/psum | solution.py:33
  109.7 41.6 %collective-permute-start.1 = (bf16[1056,384]{1,0:T(8,128)(2,1)S(1)}, bf16[1056,384]{1,0:T(8,128)(2,1)S(1)}, u32[]{:S(2)}, u32[]{:S(2)}) collective-permute-start(bf16[1056,384]{1,0:T(8,128)(2,1)S(1)} %collective-permute-done), channel_id=1, source_target_pairs={{0,4},{4,8},{8,12},{12,0},{1,5},{5,9},{9,13},{13,1},{2,6},{6,10},{... | collective-permute-start | bytes 2433032 | tf_op jit(solution)/shard_map/ppermute | solution.py:14
  151.3 32.1 %collective-permute-start.2 = (bf16[1056,384]{1,0:T(8,128)(2,1)S(1)}, bf16[1056,384]{1,0:T(8,128)(2,1)S(1)}, u32[]{:S(2)}, u32[]{:S(2)}) collective-permute-start(bf16[1056,384]{1,0:T(8,128)(2,1)S(1)} %collective-permute-done.1), channel_id=1, source_target_pairs={{0,4},{4,8},{8,12},{12,0},{1,5},{5,9},{9,13},{13,1},{2,6},{6,10},{... | collective-permute-start | bytes 2433032 | tf_op jit(solution)/shard_map/ppermute | solution.py:14
  189.7 2.1 copy-start.2
  189.7 2.1 copy-start.10
  195.4 44.9 %copy-start.11 = (f32[1056]{0:T(1024)S(1)}, f32[1056]{0:T(1024)}, u32[]{:S(2)}) copy-start(f32[1056]{0:T(1024)} %param.27) | copy-start | bytes 12676
  248.2 35.2 %copy-start.7 = (f32[1536]{0:T(1024)S(1)}, f32[1536]{0:T(1024)}, u32[]{:S(2)}) copy-start(f32[1536]{0:T(1024)} %param.29) | copy-start | bytes 18436
Sparse Core Ops, SparseCore 0:
  80.6 40.8 all-reduce.4
  248.3 33.6 all-reduce.6
Sparse Core Ops, SparseCore 1:
  82.6 93.2 all-gather.2
  177.3 63.0 all-gather.4
